TPU v7x, 32 devices: a whole 2x2x4 slice. The times are simulated.
32 devices in a mesh: sp: 16 (over z, y, x), tp: 2 (over core).
Axes of the slice: x: 2, y: 2, z: 4, core: 2. Of those that a mesh axis runs over, the one named last changes fastest.
Arguments:
- resid: bfloat16 [2048, 2048], P('sp'), may hold values from -6 to 6
- queries: bfloat16 [2048, 1024], P('sp', 'tp'), may hold values from -6 to 6
- keys: bfloat16 [2048, 1024], P('sp', 'tp'), may hold values from -6 to 6
- values: bfloat16 [2048, 2048], P('sp', 'tp'), may hold values from -6 to 6
- decay_pre: float32 [2048, 1024], P('sp', 'tp'), may hold values from -4 to 11.5
- out_gate: bfloat16 [2048, 2048], P('sp', 'tp'), may hold values from -6 to 6
- head_gain: float32 [256], replicated, may hold values from 0.1 to 1.9
- out_proj: bfloat16 [2048, 2048], P('tp'), may hold values from -0.25 to 0.25
- mix_gain: float32 [2048], replicated, may hold values from 0.1 to 1.9
- mix_shift: float32 [2048], replicated, may hold values from -3 to 3
- gate_in: bfloat16 [2048, 5632], P('sp', 'tp'), may hold values from -0.125 to 0.125
- up_in: bfloat16 [2048, 5632], P('sp', 'tp'), may hold values from -0.125 to 0.125
- down_out: bfloat16 [5632, 2048], P('tp', 'sp'), may hold values from -0.25 to 0.25
- out_gain: float32 [2048], replicated, may hold values from 0.1 to 1.9
- out_shift: float32 [2048], replicated, may hold values from -2 to 2
Outputs:
- result: bfloat16 [2048, 2048], P('sp')
All inputs are finite; a program needn't handle non-finite values.
Results may differ from a plain program's by a relative error of at most 0.02.
Values may be sent and summed in bfloat16 or wider, within the bound.
A program may use at most 128 MiB of HBM per device.

v0:
```python
import jax
import jax.numpy as jnp
from jax import lax
from jax.sharding import PartitionSpec as P

HK = 128
HV = 256
SPAN = 64
ALPHA = 2.0**0.25
LN_EPS = 1e-05
RMS_EPS = 1e-06
TAU = 16.0


def entering(array, axis, combine, identity):
    count, place = (lax.axis_size(axis), lax.axis_index(axis))
    everything = jax.tree.map(
        lambda part, kind: lax.all_gather(part.astype(kind), axis),
        array,
        (jnp.bfloat16, jnp.bfloat16),
    )
    start = jax.tree.map(
        lambda part, zero: jnp.broadcast_to(jnp.asarray(zero, part.dtype), part.shape),
        array,
        identity,
    )

    def lap(k, before):
        reached = k < place
        new = combine(
            before, jax.tree.map(lambda part, own: part[k].astype(own.dtype), everything, array)
        )
        return jax.tree.map(lambda a, b: jnp.where(reached, a, b), new, before)

    return lax.fori_loop(0, count, lap, start)


def layer_norm(inputs, gain, shift):
    center = inputs - jnp.mean(inputs, axis=-1, keepdims=True)
    spread = jnp.mean(center * center, axis=-1, keepdims=True)
    return center * lax.rsqrt(spread + LN_EPS) * gain + shift


def combine_states(earlier, later):
    return (earlier[0] * later[0], later[0][..., None] * earlier[1] + later[1])


def mix_tokens(queries, keys, values, decay_pre, out_gate, head_gain):
    tok_rows = queries.shape[0]
    local_heads = queries.shape[1] // HK
    blocks = tok_rows // SPAN
    logdecay = jax.nn.log_sigmoid(decay_pre) / TAU
    scaled_q = queries.astype(jnp.float32).reshape(blocks, SPAN, local_heads, HK) * HK ** (-0.5)
    key_block = keys.astype(jnp.float32).reshape(blocks, SPAN, local_heads, HK)
    value_block = values.astype(jnp.float32).reshape(blocks, SPAN, local_heads, HV)
    cumul = jnp.cumsum(logdecay.reshape(blocks, SPAN, local_heads, HK), axis=1)
    last = cumul[:, -1]
    key_decayed = key_block * jnp.exp(last[:, None] - cumul)
    updates = jnp.einsum(
        "nchk,nchv->nhkv", key_decayed, value_block, precision=lax.Precision.HIGHEST
    )

    def advance(running_state, inputs):
        decay_end, state_increment, current_query = inputs
        running_state = jnp.exp(decay_end)[..., None] * running_state + state_increment
        return (
            running_state,
            jnp.einsum(
                "qpy,pyr->qpr", current_query, running_state, precision=lax.Precision.HIGHEST
            ),
        )

    own_state, local_read = lax.scan(
        advance, jnp.zeros((local_heads, HK, HV), jnp.float32), (last, updates, scaled_q)
    )
    block_ends = jnp.cumsum(last, axis=0)
    own_decay = jnp.exp(block_ends[-1])
    identity = (jnp.ones_like(own_decay), jnp.zeros_like(own_state))
    _, incoming = entering((own_decay, own_state), "sp", combine_states, identity)
    carried = jnp.einsum(
        "xepj,pjw->xepw",
        scaled_q * jnp.exp(block_ends)[:, None],
        incoming,
        precision=lax.Precision.HIGHEST,
    )
    state_readout = (local_read + carried).reshape(tok_rows, local_heads, HV)
    normed = (
        state_readout
        * lax.rsqrt(jnp.mean(state_readout * state_readout, axis=-1, keepdims=True) + RMS_EPS)
        * head_gain
    )
    return (
        normed.reshape(tok_rows, local_heads * HV) * jax.nn.silu(out_gate.astype(jnp.float32))
    ).astype(jnp.bfloat16)


def hidden_by_rows(whole_rows, gate_in, up_in):
    gate = jnp.dot(
        whole_rows,
        lax.all_gather(gate_in, "sp", axis=0, tiled=True),
        preferred_element_type=jnp.float32,
    )
    upward = jnp.dot(
        whole_rows,
        lax.all_gather(up_in, "sp", axis=0, tiled=True),
        preferred_element_type=jnp.float32,
    )
    return (jax.nn.silu(gate) * upward).astype(jnp.bfloat16)


def down_by_columns(hidden, down_out):
    return jnp.dot(
        hidden,
        lax.all_gather(down_out, "sp", axis=1, tiled=True),
        preferred_element_type=jnp.float32,
    )


def body(
    resid,
    queries,
    keys,
    values,
    decay_pre,
    out_gate,
    head_gain,
    out_proj,
    mix_gain,
    mix_shift,
    gate_in,
    up_in,
    down_out,
    out_gain,
    out_shift,
):
    tp_count = lax.axis_size("tp")
    tok_rows = queries.shape[0]
    own_count = tok_rows // tp_count
    gated = mix_tokens(queries, keys, values, decay_pre, out_gate, head_gain)
    mixed = lax.psum_scatter(
        jnp.dot(gated, out_proj, preferred_element_type=jnp.float32).astype(jnp.bfloat16),
        "tp",
        scatter_dimension=0,
        tiled=True,
    ).astype(jnp.float32)
    own_resid = lax.dynamic_slice_in_dim(resid, lax.axis_index("tp") * own_count, own_count, 0)
    mid = layer_norm(ALPHA * own_resid.astype(jnp.float32) + mixed, mix_gain, mix_shift).astype(
        jnp.bfloat16
    )
    whole_rows = lax.all_gather(mid, "tp", axis=0, tiled=True)
    hidden = hidden_by_rows(whole_rows, gate_in, up_in)
    ffn = lax.psum_scatter(
        down_by_columns(hidden, down_out).astype(jnp.bfloat16),
        "tp",
        scatter_dimension=0,
        tiled=True,
    ).astype(jnp.float32)
    finished = layer_norm(ALPHA * mid.astype(jnp.float32) + 0.5 * ffn, out_gain, out_shift).astype(
        jnp.bfloat16
    )
    return lax.all_gather(finished, "tp", axis=0, tiled=True)


def solution(mesh):
    return jax.shard_map(
        body,
        mesh=mesh,
        in_specs=(
            P("sp", None),
            P("sp", "tp"),
            P("sp", "tp"),
            P("sp", "tp"),
            P("sp", "tp"),
            P("sp", "tp"),
            P(),
            P("tp", None),
            P(),
            P(),
            P("sp", "tp"),
            P("sp", "tp"),
            P("tp", "sp"),
            P(),
            P(),
        ),
        out_specs=P("sp", None),
        check_vma=False,
    )
```

profile of v0, /device:TPU:0, one launch (start us, length us, event | category | flops | bytes accessed | tf_op | source)
XLA Modules:
  0.0 625.8 jit_solution(3039727210202333603)
XLA Ops:
  11.9 1.4 while.27
  14.2 42.6 %all_gather.25 = bf16[16,4,128]{2,1,0:T(4,128)(2,1)S(1)} all-gather(bf16[1,4,128]{2,1,0:T(4,128)(2,1)S(1)} %fusion.18), channel_id=1, replica_groups=mesh['sp'=16,'tp'=2] {'sp'}, dimensions={0}, use_global_device_ids=true | all-gather | bytes 17408 | tf_op jit(solution)/shard_map/all_gather | solution.py:18
  56.8 35.8 %all-gather.12.cloned.1.call-done = bf16[64,128,256]{2,1,0:T(8,128)(2,1)} async-done(((bf16[4,128,256]{2,1,0:T(8,128)(2,1)}), bf16[64,128,256]{2,1,0:T(8,128)(2,1)}) %all-gather.12.cloned.1.call-update) | async-done | bytes 4194320 | tf_op jit(solution)/shard_map/all_gather | solution.py:18
  92.5 19.1 %while.28 = (s32[]{:T(128)}, f32[4,128,256]{2,1,0:T(8,128)S(1)}, s32[]{:T(128)}, bf16[16,4,128]{2,1,0:T(4,128)(2,1)S(1)}, bf16[16,4,128,256]{3,2,1,0:T(8,128)(2,1)}, /*index=5*/s32[]{:T(128)}, s32[]{:T(128)}) while((s32[]{:T(128)}, f32[4,128,256]{2,1,0:T(8,128)S(1)}, s32[]{:T(128)}, bf16[16,4,128]{2,1,0:T(4,128)(2,1)S(1)}, ...), condition=%wide.region_5.6_spmd.clone, body=%wide.region_4.5_spmd.clone.sunk | while | flops 655876 | bytes 1315945 | solution.py:35
  93.7 1.2 fusion.40
  94.9 1.2 fusion.40
  96.1 1.2 fusion.40
  97.3 1.2 fusion.40
  98.5 1.2 fusion.40
  99.7 1.2 fusion.40
  100.9 1.2 fusion.40
  102.1 1.2 fusion.40
  103.3 1.2 fusion.40
  104.5 1.2 fusion.40
  105.7 1.2 fusion.40
  106.9 1.2 fusion.40
  108.1 1.2 fusion.40
  109.3 1.2 fusion.40
  110.5 1.2 fusion.40
  113.4 3.8 convolution_convert_fusion.1
  119.2 4.7 reduce-scatter.3.cloned.1.call-done
  125.0 1.2 multiply_reduce_fusion.1
  127.4 2.2 all_gather.28
  129.6 139.6 %all-gather.6.cloned.1.call-done = bf16[2048,2816]{1,0:T(8,128)(2,1)} async-done(((bf16[128,2816]{1,0:T(8,128)(2,1)}), bf16[2048,2816]{1,0:T(8,128)(2,1)}) %all-gather.6.cloned.1.call-update) | async-done | bytes 11534352 | tf_op jit(solution)/shard_map/all_gather | solution.py:100
  269.2 6.0 fusion.24
  275.2 176.8 %all-gather.10.cloned.1.call-done = bf16[2816,2048]{1,0:T(8,128)(2,1)} async-done(((bf16[2816,128]{1,0:T(8,128)(2,1)}), bf16[2816,2048]{1,0:T(8,128)(2,1)}) %all-gather.10.cloned.1.call-update) | async-done | bytes 11534352 | tf_op jit(solution)/shard_map/all_gather | solution.py:114
  452.0 142.2 %all-gather.8.cloned.1.call-done = bf16[2048,2816]{1,0:T(8,128)(2,1)} async-done(((bf16[128,2816]{1,0:T(8,128)(2,1)}), bf16[2048,2816]{1,0:T(8,128)(2,1)}) %all-gather.8.cloned.1.call-update) | async-done | bytes 11534352 | tf_op jit(solution)/shard_map/all_gather | solution.py:105
  594.3 11.9 %convolution_convert_fusion = bf16[128,2048]{1,0:T(8,128)(2,1)} fusion(bf16[2816,2048]{1,0:T(8,128)(2,1)} %all-gather.10.cloned.1.call-done, bf16[128,2048]{1,0:T(8,128)(2,1)S(1)} %all_gather.28, bf16[2048,2816]{1,0:T(8,128)(2,1)} %all-gather.8.cloned.1.call-done, f32[128,2816]{1,0:T(8,128)S(1)} %fusion.24), kind=kOutput, calls=%fused_computation.12 | convolution fusion | flops 2955214848 | bytes 25559040 | tf_op jit(solution)/shard_map/dot_general | solution.py:112
  606.2 6.3 %reduce-scatter.5.cloned.1.call-done = bf16[64,2048]{1,0:T(8,128)(2,1)} async-done(((bf16[128,2048]{1,0:T(8,128)(2,1)}), bf16[64,2048]{1,0:T(8,128)(2,1)}) %reduce-scatter.5.cloned.1.call-update) | async-done | bytes 262160 | tf_op jit(solution)/shard_map/reduce_scatter | solution.py:152
  612.4 1.2 fusion.9
  613.6 1.2 multiply_reduce_fusion
  616.0 2.2 all_gather.32
  (86 shorter events, 16.4 us)
Async XLA Ops:
  6.5 7.6 %copy-start = (f32[256]{0:T(256)S(1)}, f32[256]{0:T(256)}, u32[]{:S(2)}) copy-start(f32[256]{0:T(256)} %param.25) | copy-start | bytes 3076
  6.5 86.0 %all-gather.12.cloned.1.call-start = ((), (), s32[]{:S(2)}) async-start(), calls=%async_computation.7 | async-start | bytes 4456448 | tf_op jit(solution)/shard_map/all_gather | solution.py:18
  14.0 109.9 %reduce-scatter.3.cloned.1.call-start = ((), (), s32[]{:S(2)}) async-start(), calls=%async_computation.2 | async-start | bytes 786432 | tf_op jit(solution)/shard_map/reduce_scatter | solution.py:140
  111.6 1.7 copy-start.6
  113.3 10.6 %copy-start.1 = (bf16[128,2048]{1,0:T(8,128)(2,1)S(1)}, bf16[128,2048]{1,0:T(8,128)(2,1)}, u32[]{:S(2)}) copy-start(bf16[128,2048]{1,0:T(8,128)(2,1)} %param.19) | copy-start | bytes 1572868
  113.3 12.9 %copy-start.2 = (f32[2048]{0:T(1024)S(1)}, f32[2048]{0:T(1024)}, u32[]{:S(2)}) copy-start(f32[2048]{0:T(1024)} %param.28) | copy-start | bytes 24580
  113.3 12.9 %copy-start.3 = (f32[2048]{0:T(1024)S(1)}, f32[2048]{0:T(1024)}, u32[]{:S(2)}) copy-start(f32[2048]{0:T(1024)} %param.27) | copy-start | bytes 24580
  117.2 152.0 %all-gather.6.cloned.1.call-start = ((), (), s32[]{:S(2)}) async-start(), calls=%async_computation.3 | async-start | bytes 12255232 | tf_op jit(solution)/shard_map/all_gather | solution.py:100
  118.0 334.1 %all-gather.10.cloned.1.call-start = ((), (), s32[]{:S(2)}) async-start(), calls=%async_computation.5 | async-start | bytes 12255232 | tf_op jit(solution)/shard_map/all_gather | solution.py:114
  118.5 475.7 %all-gather.8.cloned.1.call-start = ((), (), s32[]{:S(2)}) async-start(), calls=%async_computation.4 | async-start | bytes 12255232 | tf_op jit(solution)/shard_map/all_gather | solution.py:105
  119.1 493.3 %reduce-scatter.5.cloned.1.call-start = ((), (), s32[]{:S(2)}) async-start(), calls=%async_computation.6 | async-start | bytes 786432 | tf_op jit(solution)/shard_map/reduce_scatter | solution.py:152
  275.2 339.6 %copy-start.4 = (f32[2048]{0:T(1024)S(1)}, f32[2048]{0:T(1024)}, u32[]{:S(2)}) copy-start(f32[2048]{0:T(1024)} %param.33) | copy-start | bytes 24580
  275.2 339.6 %copy-start.5 = (f32[2048]{0:T(1024)S(1)}, f32[2048]{0:T(1024)}, u32[]{:S(2)}) copy-start(f32[2048]{0:T(1024)} %param.32) | copy-start | bytes 24580
Sparse Core Ops, SparseCore 0:
  14.1 78.3 all-gather.11
  117.3 6.5 reduce-scatter.2
  126.7 142.5 all-gather.5
  271.8 180.2 all-gather.9
  454.6 139.5 all-gather.7
  606.3 6.0 reduce-scatter.4
where the time goes:
time: 627 us; the launch traced here: 626 us
  waiting for transfers between devices  507 us (81%)
  blocking collectives  47 us (7%)
  other arithmetic  28.2 us (4%)
  matrix products  23.8 us (4%)
  between operations  13.8 us (2%)
    all_gather x1, waiting for transfers between devices, down_by_columns(): lax.all_gather(down_out, 'sp', axis=1, tiled=True)  177 us
    all_gather x1, waiting for transfers between devices, hidden_by_rows(): lax.all_gather(up_in, 'sp', axis=0, tiled=True)  142 us
    all_gather x1, waiting for transfers between devices, hidden_by_rows(): lax.all_gather(gate_in, 'sp', axis=0, tiled=True)  140 us
    all_gather x1, blocking collectives, entering(): lax.all_gather(part.astype(kind), axis)  42.6 us
    all_gather x1, waiting for transfers between devices, entering(): lax.all_gather(part.astype(kind), axis)  35.8 us
    select_n x16, other arithmetic, lap(): return jax.tree.map(lambda a, b: jnp.where(reached, a, b), new, before)  18.4 us
  transfers between devices with their start and end apart: 6, of which 6 were waited for; matrix products, arithmetic and copies ran while one was open for 2% of the time, Pallas kernels for 0%

commit v1 on v0

--- a/solution.py
+++ b/solution.py
@@ -10,6 +10,10 @@
 LN_EPS = 1e-05
 RMS_EPS = 1e-06
 TAU = 16.0
+
+
+def _guide_modes(packet, mesh_ax, axis_no):
+    return jnp.concatenate(lax.all_gather(packet, axis_name=mesh_ax), axis_no)
 
 
 def entering(array, axis, combine, identity):
@@ -109,11 +113,7 @@
 
 
 def down_by_columns(hidden, down_out):
-    return jnp.dot(
-        hidden,
-        lax.all_gather(down_out, "sp", axis=1, tiled=True),
-        preferred_element_type=jnp.float32,
-    )
+    return jnp.dot(hidden, _guide_modes(down_out, "sp", 1), preferred_element_type=jnp.float32)
 
 
 def body(

time: 627 us -> 588 us (0.938)
  waiting for transfers between devices: 507 us -> 451 us
  local copies, waits for them, and re-layouts: 4.97 us -> 20.2 us
    all_gather x1, waiting for transfers between devices: 177 us -> 139 us  [_guide_modes(): return jnp.concatenate(lax.all_gather(packet, axis_name=mesh_ax), axis_no)]
    reshape x0 -> x1, local copies, waits for them, and re-layouts: none -> 15.2 us  [_guide_modes(): return jnp.concatenate(lax.all_gather(packet, axis_name=mesh_ax), axis_no)]
    all_gather x1, waiting for transfers between devices: 140 us -> 127 us  [hidden_by_rows(): lax.all_gather(gate_in, 'sp', axis=0, tiled=True)]
  transfers between devices with their start and end apart: 6 -> 6, of which waited for: 6 -> 6; matrix products, arithmetic and copies ran while one was open for 2% -> 4% of each run, Pallas kernels for 0% -> 0%
where the time goes in v1:
time: 588 us; the launch traced here: 587 us
  waiting for transfers between devices  451 us (77%)
  blocking collectives  47.1 us (8%)
  other arithmetic  28.2 us (5%)
  matrix products  25.2 us (4%)
  local copies, waits for them, and re-layouts  20.2 us (3%)
  between operations  13.8 us (2%)
    all_gather x1, waiting for transfers between devices, _guide_modes(): return jnp.concatenate(lax.all_gather(packet, axis_name=mesh_ax), axis_no)  139 us
    all_gather x1, waiting for transfers between devices, hidden_by_rows(): lax.all_gather(up_in, 'sp', axis=0, tiled=True)  136 us
    all_gather x1, waiting for transfers between devices, hidden_by_rows(): lax.all_gather(gate_in, 'sp', axis=0, tiled=True)  127 us
    all_gather x1, blocking collectives, entering(): lax.all_gather(part.astype(kind), axis)  42.6 us
    all_gather x1, waiting for transfers between devices, entering(): lax.all_gather(part.astype(kind), axis)  35.8 us
    select_n x16, other arithmetic, lap(): return jax.tree.map(lambda a, b: jnp.where(reached, a, b), new, before)  18.4 us
    reshape x1, local copies, waits for them, and re-layouts, _guide_modes(): return jnp.concatenate(lax.all_gather(packet, axis_name=mesh_ax), axis_no)  15.2 us
    dot_general x1, matrix products, down_by_columns(): jnp.dot(hidden, _guide_modes(down_out, 'sp', 1), preferred_element_type=j...  13.3 us
  transfers between devices with their start and end apart: 6, of which 6 were waited for; matrix products, arithmetic and copies ran while one was open for 4% of the time, Pallas kernels for 0%

profile of v1, /device:TPU:0, one launch (start us, length us, event | category | flops | bytes accessed | tf_op | source)
XLA Modules:
  0.0 586.6 jit_solution(4975677808484829431)
XLA Ops:
  11.9 1.4 while.27
  14.2 42.6 %all_gather.28 = bf16[16,4,128]{2,1,0:T(4,128)(2,1)S(1)} all-gather(bf16[1,4,128]{2,1,0:T(4,128)(2,1)S(1)} %fusion.18), channel_id=1, replica_groups=mesh['sp'=16,'tp'=2] {'sp'}, dimensions={0}, use_global_device_ids=true | all-gather | bytes 17408 | tf_op jit(solution)/shard_map/all_gather | solution.py:22
  56.8 35.8 %all-gather.11.cloned.1.call-done = bf16[64,128,256]{2,1,0:T(8,128)(2,1)} async-done(((bf16[4,128,256]{2,1,0:T(8,128)(2,1)}), bf16[64,128,256]{2,1,0:T(8,128)(2,1)}) %all-gather.11.cloned.1.call-update) | async-done | bytes 4194320 | tf_op jit(solution)/shard_map/all_gather | solution.py:22
  92.5 19.1 %while.28 = (s32[]{:T(128)}, f32[4,128,256]{2,1,0:T(8,128)S(1)}, s32[]{:T(128)}, bf16[16,4,128]{2,1,0:T(4,128)(2,1)S(1)}, bf16[16,4,128,256]{3,2,1,0:T(8,128)(2,1)}, /*index=5*/s32[]{:T(128)}, s32[]{:T(128)}) while((s32[]{:T(128)}, f32[4,128,256]{2,1,0:T(8,128)S(1)}, s32[]{:T(128)}, bf16[16,4,128]{2,1,0:T(4,128)(2,1)S(1)}, ...), condition=%wide.region_5.6_spmd.clone, body=%wide.region_4.5_spmd.clone.sunk | while | flops 655876 | bytes 1315945 | solution.py:39
  93.7 1.2 fusion.40
  94.9 1.2 fusion.40
  96.1 1.2 fusion.40
  97.3 1.2 fusion.40
  98.5 1.2 fusion.40
  99.7 1.2 fusion.40
  100.9 1.2 fusion.40
  102.1 1.2 fusion.40
  103.3 1.2 fusion.40
  104.5 1.2 fusion.40
  105.7 1.2 fusion.40
  106.9 1.2 fusion.40
  108.1 1.2 fusion.40
  109.3 1.2 fusion.40
  110.5 1.2 fusion.40
  113.4 3.8 convolution_convert_fusion.1
  119.2 4.7 reduce-scatter.3.cloned.1.call-done
  125.1 1.2 multiply_reduce_fusion.1
  127.4 2.4 all_gather.31
  129.8 139.5 %all-gather.13.cloned.1.call-done = bf16[45056,128]{1,0:T(8,128)(2,1)} async-done(((bf16[2816,128]{1,0:T(8,128)(2,1)}), bf16[45056,128]{1,0:T(8,128)(2,1)}) %all-gather.13.cloned.1.call-update) | async-done | bytes 11534352 | tf_op jit(solution)/shard_map/all_gather | solution.py:16
  269.2 15.2 %copy.40 = bf16[2816,16,128]{0,2,1:T(8,128)(2,1)} copy(bf16[2816,16,128]{2,0,1:T(8,128)(2,1)} %bitcast.70) | data formatting | bytes 23068672 | tf_op jit(solution)/shard_map/reshape | solution.py:16
  284.4 127.1 %all-gather.7.cloned.1.call-done = bf16[2048,2816]{1,0:T(8,128)(2,1)} async-done(((bf16[128,2816]{1,0:T(8,128)(2,1)}), bf16[2048,2816]{1,0:T(8,128)(2,1)}) %all-gather.7.cloned.1.call-update) | async-done | bytes 11534352 | tf_op jit(solution)/shard_map/all_gather | solution.py:104
  411.5 6.0 %fusion.24 = f32[128,2816]{1,0:T(8,128)S(1)} fusion(bf16[128,2048]{1,0:T(8,128)(2,1)S(1)} %all_gather.31, bf16[2048,2816]{1,0:T(8,128)(2,1)} %all-gather.7.cloned.1.call-done), kind=kOutput, calls=%fused_computation.56 | convolution fusion | flops 1476395008 | bytes 13500416 | tf_op jit(solution)/shard_map/dot_general | solution.py:102
  417.4 136.3 %all-gather.9.cloned.1.call-done = bf16[2048,2816]{1,0:T(8,128)(2,1)} async-done(((bf16[128,2816]{1,0:T(8,128)(2,1)}), bf16[2048,2816]{1,0:T(8,128)(2,1)}) %all-gather.9.cloned.1.call-update) | async-done | bytes 11534352 | tf_op jit(solution)/shard_map/all_gather | solution.py:109
  553.7 13.3 %convolution_convert_fusion = bf16[128,2048]{1,0:T(8,128)(2,1)} fusion(bf16[2816,2048]{0,1:T(8,128)(2,1)} %bitcast.71, bf16[128,2048]{1,0:T(8,128)(2,1)S(1)} %all_gather.31, bf16[2048,2816]{1,0:T(8,128)(2,1)} %all-gather.9.cloned.1.call-done, f32[128,2816]{1,0:T(8,128)S(1)} %fusion.24), kind=kOutput, calls=%fused_computation.12 | convolution fusion | flops 2955214848 | bytes 25559040 | tf_op jit(solution)/shard_map/dot_general | solution.py:116
  567.0 6.3 %reduce-scatter.5.cloned.1.call-done = bf16[64,2048]{1,0:T(8,128)(2,1)} async-done(((bf16[128,2048]{1,0:T(8,128)(2,1)}), bf16[64,2048]{1,0:T(8,128)(2,1)}) %reduce-scatter.5.cloned.1.call-update) | async-done | bytes 262160 | tf_op jit(solution)/shard_map/reduce_scatter | solution.py:152
  574.4 1.2 multiply_reduce_fusion
  576.8 2.2 all_gather.36
  (89 shorter events, 17.6 us)
Async XLA Ops:
  6.5 7.6 %copy-start = (f32[256]{0:T(256)S(1)}, f32[256]{0:T(256)}, u32[]{:S(2)}) copy-start(f32[256]{0:T(256)} %param.25) | copy-start | bytes 3076
  6.5 86.0 %all-gather.11.cloned.1.call-start = ((), (), s32[]{:S(2)}) async-start(), calls=%async_computation.6 | async-start | bytes 4456448 | tf_op jit(solution)/shard_map/all_gather | solution.py:22
  14.0 109.9 %reduce-scatter.3.cloned.1.call-start = ((), (), s32[]{:S(2)}) async-start(), calls=%async_computation.2 | async-start | bytes 786432 | tf_op jit(solution)/shard_map/reduce_scatter | solution.py:140
  111.6 1.7 copy-start.7
  113.3 10.6 %copy-start.2 = (bf16[128,2048]{1,0:T(8,128)(2,1)S(1)}, bf16[128,2048]{1,0:T(8,128)(2,1)}, u32[]{:S(2)}) copy-start(bf16[128,2048]{1,0:T(8,128)(2,1)} %param.19) | copy-start | bytes 1572868
  113.3 12.9 %copy-start.3 = (f32[2048]{0:T(1024)S(1)}, f32[2048]{0:T(1024)}, u32[]{:S(2)}) copy-start(f32[2048]{0:T(1024)} %param.28) | copy-start | bytes 24580
  113.3 12.9 %copy-start.4 = (f32[2048]{0:T(1024)S(1)}, f32[2048]{0:T(1024)}, u32[]{:S(2)}) copy-start(f32[2048]{0:T(1024)} %param.27) | copy-start | bytes 24580
  117.2 152.0 %all-gather.13.cloned.1.call-start = ((), (), s32[]{:S(2)}) async-start(), calls=%async_computation.7 | async-start | bytes 12255232 | tf_op jit(solution)/shard_map/all_gather | solution.py:16
  118.0 293.5 %all-gather.7.cloned.1.call-start = ((), (), s32[]{:S(2)}) async-start(), calls=%async_computation.3 | async-start | bytes 12255232 | tf_op jit(solution)/shard_map/all_gather | solution.py:104
  118.5 435.2 %all-gather.9.cloned.1.call-start = ((), (), s32[]{:S(2)}) async-start(), calls=%async_computation.4 | async-start | bytes 12255232 | tf_op jit(solution)/shard_map/all_gather | solution.py:109
  119.1 454.1 %reduce-scatter.5.cloned.1.call-start = ((), (), s32[]{:S(2)}) async-start(), calls=%async_computation.5 | async-start | bytes 786432 | tf_op jit(solution)/shard_map/reduce_scatter | solution.py:152
  553.7 21.9 %copy-start.5 = (f32[2048]{0:T(1024)S(1)}, f32[2048]{0:T(1024)}, u32[]{:S(2)}) copy-start(f32[2048]{0:T(1024)} %param.33) | copy-start | bytes 24580
  553.7 21.9 %copy-start.6 = (f32[2048]{0:T(1024)S(1)}, f32[2048]{0:T(1024)}, u32[]{:S(2)}) copy-start(f32[2048]{0:T(1024)} %param.32) | copy-start | bytes 24580
  553.7 26.1 %copy-start.1 = (f32[256]{0:T(256)S(1)}, f32[256]{0:T(256)}, u32[]{:S(2)}) copy-start(f32[256]{0:T(256)} %param.25) | copy-start | bytes 3076
Sparse Core Ops, SparseCore 0:
  14.1 78.3 all-gather.10
  117.3 6.5 reduce-scatter.2
  126.7 142.5 all-gather.12
  271.8 139.5 all-gather.6
  414.1 139.5 all-gather.8
  567.1 6.0 reduce-scatter.4
